TPU v7x, 32 devices: a whole 2x2x4 slice. The times are simulated.
32 devices in a mesh: fs: 4 (over y, x), tp: 8 (over z, core).
Axes of the slice: x: 2, y: 2, z: 4, core: 2. Of those that a mesh axis runs over, the one named last changes fastest.
Arguments:
- stream_in: bfloat16 [4096, 4096], P(('fs', 'tp')), may hold values from -6 to 6
- mixer_out: bfloat16 [4096, 4096], P(('fs', 'tp')), may hold values from -6 to 6
- mix_gain: float32 [4096], replicated, may hold values from 0.1 to 1.9
- pre_gain: float32 [4096], replicated, may hold values from 0.1 to 1.9
- gate_weight: float32 [4096, 6144], P('fs', 'tp'), may hold values from -0.09375 to 0.09375
- up_weight: float32 [4096, 6144], P('fs', 'tp'), may hold values from -0.09375 to 0.09375
- gate_scale: float32 [6144], P('tp'), may hold values from 0.5 to 2
- up_scale: float32 [6144], P('tp'), may hold values from 0.5 to 2
Outputs:
- hidden: bfloat16 [4096, 6144], P('fs', 'tp')
- stream: bfloat16 [4096, 4096], P(('fs', 'tp'))
All inputs are finite; a program needn't handle non-finite values.
Results may differ from a plain program's by a relative error of at most 0.0082.
Values may be sent and summed in bfloat16 or wider, within the bound.
A program may use at most 128 MiB of HBM per device.

v0:
```python
import jax
import jax.numpy as jnp
from jax import lax
from jax.sharding import PartitionSpec as P

epsilon = 1e-06


def rms_scaled(values, gain):
    return values * lax.rsqrt(jnp.mean(values * values, axis=-1, keepdims=True) + epsilon) * gain


def on_device(
    stream_in, mixer_out, mix_gain, pre_gain, gate_weight, up_weight, gate_scale, up_scale
):
    mixed = stream_in.astype(jnp.float32) + rms_scaled(mixer_out.astype(jnp.float32), mix_gain)
    stream = mixed.astype(jnp.bfloat16)
    normed = rms_scaled(stream.astype(jnp.float32), pre_gain).astype(jnp.bfloat16)
    gate_cast = gate_weight.astype(jnp.bfloat16)
    up_cast = up_weight.astype(jnp.bfloat16)
    gate_full, up_full = (
        lax.all_gather(gate_cast, "fs", axis=0, tiled=True),
        lax.all_gather(up_cast, "fs", axis=0, tiled=True),
    )
    piece = lax.all_gather(normed, "tp", axis=0, tiled=True)
    gate = jnp.dot(piece, gate_full, preferred_element_type=jnp.float32) * gate_scale
    up = jnp.dot(piece, up_full, preferred_element_type=jnp.float32) * up_scale
    hidden = (jax.nn.silu(gate) * up).astype(jnp.bfloat16)
    return (hidden, stream)


def solution(mesh):
    return jax.shard_map(
        on_device,
        mesh=mesh,
        in_specs=(
            P(("fs", "tp"), None),
            P(("fs", "tp"), None),
            P(),
            P(),
            P("fs", "tp"),
            P("fs", "tp"),
            P("tp"),
            P("tp"),
        ),
        out_specs=(P("fs", "tp"), P(("fs", "tp"), None)),
        check_vma=False,
    )
```

profile of v0, /device:TPU:0, one launch (start us, length us, event | category | flops | bytes accessed | tf_op | source)
XLA Modules:
  0.0 256.1 jit_solution(6884719773406794379)
XLA Ops:
  7.2 0.0 copy-start.1
  7.2 0.0 copy-start.3
  7.2 0.0 copy-start.2
  7.2 0.0 all-gather.6.cloned.1.call-start
  7.2 3.3 %convert_element_type.29 = bf16[1024,768]{1,0:T(8,128)(2,1)} convert(f32[1024,768]{1,0:T(8,128)} %param.12) | non-fusion elementwise | flops 786432 | bytes 4718592 | tf_op jit(solution)/shard_map/convert_element_type | solution.py:19
  10.6 0.0 copy-start.4
  10.6 0.0 all-gather.6.cloned.1.call-update
  10.6 0.0 all-gather.4.cloned.1.call-start
  10.6 0.0 copy-done.1
  10.6 0.3 fusion
  10.9 0.0 copy-done.3
  11.0 0.0 copy-done.2
  11.0 0.7 fusion.4
  11.7 0.0 copy-start
  11.7 0.0 copy-done.4
  11.7 1.3 fusion.6
  13.1 0.0 all-gather.4.cloned.1.call-update
  13.1 0.0 all-gather.8.cloned.1.call-start
  13.2 3.2 %convert_element_type.30 = bf16[1024,768]{1,0:T(8,128)(2,1)} convert(f32[1024,768]{1,0:T(8,128)} %param.13) | non-fusion elementwise | flops 786432 | bytes 4718592 | tf_op jit(solution)/shard_map/convert_element_type | solution.py:20
  16.4 0.0 copy-done
  16.4 0.0 all-gather.8.cloned.1.call-update
  16.4 0.0 copy-start.5
  16.4 0.0 copy-start.6
  16.4 67.1 %all-gather.6.cloned.1.call-done = bf16[4096,768]{1,0:T(8,128)(2,1)} async-done(((bf16[1024,768]{1,0:T(8,128)(2,1)}), bf16[4096,768]{1,0:T(8,128)(2,1)}) %all-gather.6.cloned.1.call-update) | async-done | bytes 6291472 | tf_op jit(solution)/shard_map/all_gather | solution.py:22
  83.5 83.7 %all-gather.4.cloned.1.call-done = bf16[1024,4096]{1,0:T(8,128)(2,1)} async-done(((bf16[128,4096]{1,0:T(8,128)(2,1)}), bf16[1024,4096]{1,0:T(8,128)(2,1)}) %all-gather.4.cloned.1.call-update) | async-done | bytes 8388624 | tf_op jit(solution)/shard_map/all_gather | solution.py:25
  167.2 10.9 %fusion.8 = f32[1024,768]{1,0:T(8,128)S(1)} fusion(bf16[1024,4096]{1,0:T(8,128)(2,1)} %all-gather.4.cloned.1.call-done, bf16[4096,768]{1,0:T(8,128)(2,1)} %all-gather.6.cloned.1.call-done), kind=kOutput, calls=%fused_computation.14 | convolution fusion | flops 6442450944 | bytes 17825792 | tf_op jit(solution)/shard_map/dot_general | solution.py:26
  178.1 59.5 %all-gather.8.cloned.1.call-done = bf16[4096,768]{1,0:T(8,128)(2,1)} async-done(((bf16[1024,768]{1,0:T(8,128)(2,1)}), bf16[4096,768]{1,0:T(8,128)(2,1)}) %all-gather.8.cloned.1.call-update) | async-done | bytes 6291472 | tf_op jit(solution)/shard_map/all_gather | solution.py:23
  237.6 0.0 copy-done.5
  237.6 0.0 copy-done.6
  237.6 12.1 %multiply_convert_fusion = bf16[1024,768]{1,0:T(8,128)(2,1)} fusion(f32[1024,768]{1,0:T(8,128)S(1)} %fusion.8, bf16[1024,4096]{1,0:T(8,128)(2,1)} %all-gather.4.cloned.1.call-done, bf16[4096,768]{1,0:T(8,128)(2,1)} %all-gather.8.cloned.1.call-done, f32[768]{0:T(1024)S(1)} %copy-done.5, f32[768]{0:T(1024)S(1)} %copy-done.6), kind=kOutput, calls=%fused_computation | convolution fusion | flops 6448742400 | bytes 19404800 | tf_op jit(solution)/shard_map/dot_general | solution.py:27
  (2 shorter events, 0.0 us)
Async XLA Ops:
  7.2 3.5 %copy-start.1 = (bf16[128,4096]{1,0:T(8,128)(2,1)S(1)}, bf16[128,4096]{1,0:T(8,128)(2,1)}, u32[]{:S(2)}) copy-start(bf16[128,4096]{1,0:T(8,128)(2,1)} %param.9) | copy-start | bytes 3145732
  7.2 3.8 %copy-start.3 = (f32[4096]{0:T(1024)S(1)}, f32[4096]{0:T(1024)}, u32[]{:S(2)}) copy-start(f32[4096]{0:T(1024)} %param.10) | copy-start | bytes 49156
  7.2 3.8 %copy-start.2 = (bf16[128,4096]{1,0:T(8,128)(2,1)S(1)}, bf16[128,4096]{1,0:T(8,128)(2,1)}, u32[]{:S(2)}) copy-start(bf16[128,4096]{1,0:T(8,128)(2,1)} %param.8) | copy-start | bytes 3145732
  7.2 76.3 %all-gather.6.cloned.1.call-start = ((), (), s32[]{:S(2)}) async-start(), calls=%async_computation.1 | async-start | bytes 7864320 | tf_op jit(solution)/shard_map/all_gather | solution.py:22
  10.6 1.2 copy-start.4
  10.6 156.6 %all-gather.4.cloned.1.call-start = ((), (), s32[]{:S(2)}) async-start(), calls=%async_computation | async-start | bytes 9437184 | tf_op jit(solution)/shard_map/all_gather | solution.py:25
  11.7 4.7 %copy-start = (bf16[128,4096]{1,0:T(8,128)(2,1)}, bf16[128,4096]{1,0:T(8,128)(2,1)S(1)}, u32[]{:S(2)}) copy-start(bf16[128,4096]{1,0:T(8,128)(2,1)S(1)} %get-tuple-element.3) | copy-start | bytes 3145732
  13.1 224.4 %all-gather.8.cloned.1.call-start = ((), (), s32[]{:S(2)}) async-start(), calls=%async_computation.2 | async-start | bytes 7864320 | tf_op jit(solution)/shard_map/all_gather | solution.py:23
  16.4 221.2 %copy-start.5 = (f32[768]{0:T(1024)S(1)}, f32[768]{0:T(1024)}, u32[]{:S(2)}) copy-start(f32[768]{0:T(1024)} %param.15) | copy-start | bytes 9220
  16.4 221.1 %copy-start.6 = (f32[768]{0:T(1024)S(1)}, f32[768]{0:T(1024)}, u32[]{:S(2)}) copy-start(f32[768]{0:T(1024)} %param.14) | copy-start | bytes 9220
Sparse Core Ops, SparseCore 0:
  10.7 72.7 all-gather.5
  85.1 82.0 all-gather.3
  169.0 68.5 all-gather.7
where the time goes:
time: 256 us
  waiting for transfers between devices  210 us (82%)
  matrix products  23 us (9%)
  between operations  13.8 us (5%)
  other arithmetic  8.92 us (3%)
    all_gather x1, waiting for transfers between devices, on_device(): piece = lax.all_gather(normed, 'tp', axis=0, tiled=True)  83.7 us
    all_gather x1, waiting for transfers between devices, on_device(): lax.all_gather(gate_cast, 'fs', axis=0, tiled=True)  67.1 us
    all_gather x1, waiting for transfers between devices, on_device(): lax.all_gather(up_cast, 'fs', axis=0, tiled=True)  59.5 us
    dot_general x1, matrix products, on_device(): up = jnp.dot(piece, up_full, preferred_element_type=jnp.float32) * up_scale  12.1 us
    dot_general x1, matrix products, on_device(): jnp.dot(piece, gate_full, preferred_element_type=jnp.float32) * gate_scale  10.9 us
  transfers between devices with their start and end apart: 3, of which 3 were waited for; matrix products, arithmetic and copies ran while one was open for 6% of the time, Pallas kernels for 0%

commit v1 on v0

--- a/solution.py
+++ b/solution.py
@@ -22,7 +22,9 @@
         lax.all_gather(gate_cast, "fs", axis=0, tiled=True),
         lax.all_gather(up_cast, "fs", axis=0, tiled=True),
     )
-    piece = lax.all_gather(normed, "tp", axis=0, tiled=True)
+    piece = jnp.concatenate(
+        lax.all_to_all(jnp.stack([normed for _ in range(lax.axis_size("tp"))]), "tp", 0, 0), axis=0
+    )
     gate = jnp.dot(piece, gate_full, preferred_element_type=jnp.float32) * gate_scale
     up = jnp.dot(piece, up_full, preferred_element_type=jnp.float32) * up_scale
     hidden = (jax.nn.silu(gate) * up).astype(jnp.bfloat16)

time: 256 us -> 237 us (0.926)
  waiting for transfers between devices: 210 us -> 180 us
  starting transfers between devices: 0.12 us -> 6.43 us
  local copies, waits for them, and re-layouts: 0.04 us -> 4.32 us
    all_to_all x0 -> x1, waiting for transfers between devices: none -> 123 us  [on_device(): lax.all_to_all(jnp.stack([normed for _ in range(lax.axis_size('tp'))]), '...]
    all_gather x1 -> x0, waiting for transfers between devices: 83.7 us -> none  [on_device(): piece = lax.all_gather(normed, 'tp', axis=0, tiled=True)]
    all_gather x1, waiting for transfers between devices: 59.5 us -> 0.02 us  [on_device(): lax.all_gather(up_cast, 'fs', axis=0, tiled=True)]
    all_gather x1, waiting for transfers between devices: 67.1 us -> 57.1 us  [on_device(): lax.all_gather(gate_cast, 'fs', axis=0, tiled=True)]
    all_to_all x0 -> x1, starting transfers between devices: none -> 6.35 us  [on_device(): lax.all_to_all(jnp.stack([normed for _ in range(lax.axis_size('tp'))]), '...]
    another operation x0 -> x1, local copies, waits for them, and re-layouts: none -> 4.29 us  [on_device(): jnp.stack([normed for _ in range(lax.axis_size('tp'))])]
  transfers between devices with their start and end apart: 3 -> 3, of which waited for: 3 -> 2; matrix products, arithmetic and copies ran while one was open for 6% -> 9% of each run, Pallas kernels for 0% -> 0%
where the time goes in v1:
time: 237 us
  waiting for transfers between devices  180 us (76%)
  matrix products  23 us (10%)
  between operations  14.2 us (6%)
  other arithmetic  8.35 us (4%)
  starting transfers between devices  6.43 us (3%)
  local copies, waits for them, and re-layouts  4.32 us (2%)
    all_to_all x1, waiting for transfers between devices, on_device(): lax.all_to_all(jnp.stack([normed for _ in range(lax.axis_size('tp'))]), '...  123 us
    all_gather x1, waiting for transfers between devices, on_device(): lax.all_gather(gate_cast, 'fs', axis=0, tiled=True)  57.1 us
    dot_general x1, matrix products, on_device(): up = jnp.dot(piece, up_full, preferred_element_type=jnp.float32) * up_scale  12.1 us
    dot_general x1, matrix products, on_device(): jnp.dot(piece, gate_full, preferred_element_type=jnp.float32) * gate_scale  10.9 us
    all_to_all x1, starting transfers between devices, on_device(): lax.all_to_all(jnp.stack([normed for _ in range(lax.axis_size('tp'))]), '...  6.35 us
  transfers between devices with their start and end apart: 3, of which 2 were waited for; matrix products, arithmetic and copies ran while one was open for 9% of the time, Pallas kernels for 0%

profile of v1, /device:TPU:0, one launch (start us, length us, event | category | flops | bytes accessed | tf_op | source)
XLA Modules:
  0.0 236.5 jit_solution(17534407387343520380)
XLA Ops:
  7.2 0.0 copy-start.1
  7.2 0.0 copy-start.3
  7.2 0.0 copy-start.2
  7.2 0.0 all-gather.3.cloned.1.call-start
  7.2 3.3 %convert_element_type.29 = bf16[1024,768]{1,0:T(8,128)(2,1)} convert(f32[1024,768]{1,0:T(8,128)} %param.12) | non-fusion elementwise | flops 786432 | bytes 4718592 | tf_op jit(solution)/shard_map/convert_element_type | solution.py:19
  10.6 0.0 copy-start.4
  10.6 0.0 all-gather.3.cloned.1.call-update
  10.6 0.0 copy-done.1
  10.6 0.3 fusion
  10.9 0.0 copy-done.3
  10.9 0.0 copy-done.2
  10.9 0.7 fusion.4
  11.7 0.0 copy-start
  11.7 0.0 copy-done.4
  11.7 0.3 fusion.6
  12.0 4.3 %stack.2 = bf16[8,128,4096]{2,1,0:T(8,128)(2,1)} broadcast(bf16[128,4096]{1,0:T(8,128)(2,1)S(1)} %fusion.6), dimensions={1,2} | broadcast | bytes 9437184 | tf_op jit(solution)/shard_map/stack | solution.py:26
  16.3 0.0 copy-done
  16.3 6.4 %all-to-all-start = ((bf16[8,128,4096]{2,1,0:T(8,128)(2,1)}), bf16[8,128,4096]{2,1,0:T(8,128)(2,1)}, u32[]{:S(2)}, u32[]{:S(2)}) async-start(bf16[8,128,4096]{2,1,0:T(8,128)(2,1)} %stack.2), calls=%async_computation | async-start | bytes 16777216 | tf_op jit(solution)/shard_map/all_to_all | solution.py:26
  22.7 0.0 all-gather.5.cloned.1.call-start
  22.7 3.7 %convert_element_type.30 = bf16[1024,768]{1,0:T(8,128)(2,1)} convert(f32[1024,768]{1,0:T(8,128)} %param.13) | non-fusion elementwise | flops 786432 | bytes 4718592 | tf_op jit(solution)/shard_map/convert_element_type | solution.py:20
  26.4 0.0 all-gather.5.cloned.1.call-update
  26.4 57.1 %all-gather.3.cloned.1.call-done = bf16[4096,768]{1,0:T(8,128)(2,1)} async-done(((bf16[1024,768]{1,0:T(8,128)(2,1)}), bf16[4096,768]{1,0:T(8,128)(2,1)}) %all-gather.3.cloned.1.call-update) | async-done | bytes 6291472 | tf_op jit(solution)/shard_map/all_gather | solution.py:22
  83.5 123.1 %all-to-all-done = bf16[8,128,4096]{2,1,0:T(8,128)(2,1)} async-done(((bf16[8,128,4096]{2,1,0:T(8,128)(2,1)}), bf16[8,128,4096]{2,1,0:T(8,128)(2,1)}, u32[]{:S(2)}, u32[]{:S(2)}) %all-to-all-start) | async-done | bytes 8388640 | tf_op jit(solution)/shard_map/all_to_all | solution.py:26
  206.6 0.0 copy-start.5
  206.6 0.0 copy-start.6
  206.6 10.9 %fusion.8 = f32[1024,768]{1,0:T(8,128)S(1)} fusion(bf16[1024,4096]{1,0:T(8,128)(2,1)} %bitcast, bf16[4096,768]{1,0:T(8,128)(2,1)} %all-gather.3.cloned.1.call-done), kind=kOutput, calls=%fused_computation.14 | convolution fusion | flops 6442450944 | bytes 17825792 | tf_op jit(solution)/shard_map/dot_general | solution.py:28
  217.6 0.0 all-gather.5.cloned.1.call-done
  217.6 0.0 copy-done.5
  217.6 0.0 copy-done.6
  217.6 12.1 %multiply_convert_fusion = bf16[1024,768]{1,0:T(8,128)(2,1)} fusion(f32[1024,768]{1,0:T(8,128)S(1)} %fusion.8, bf16[1024,4096]{1,0:T(8,128)(2,1)} %bitcast, bf16[4096,768]{1,0:T(8,128)(2,1)} %all-gather.5.cloned.1.call-done, f32[768]{0:T(1024)S(1)} %copy-done.5, f32[768]{0:T(1024)S(1)} %copy-done.6), kind=kOutput, calls=%fused_computation | convolution fusion | flops 6448742400 | bytes 19404800 | tf_op jit(solution)/shard_map/dot_general | solution.py:29
  (2 shorter events, 0.0 us)
Async XLA Ops:
  7.2 3.4 %copy-start.1 = (bf16[128,4096]{1,0:T(8,128)(2,1)S(1)}, bf16[128,4096]{1,0:T(8,128)(2,1)}, u32[]{:S(2)}) copy-start(bf16[128,4096]{1,0:T(8,128)(2,1)} %param.9) | copy-start | bytes 3145732
  7.2 3.7 %copy-start.3 = (f32[4096]{0:T(1024)S(1)}, f32[4096]{0:T(1024)}, u32[]{:S(2)}) copy-start(f32[4096]{0:T(1024)} %param.10) | copy-start | bytes 49156
  7.2 3.7 %copy-start.2 = (bf16[128,4096]{1,0:T(8,128)(2,1)S(1)}, bf16[128,4096]{1,0:T(8,128)(2,1)}, u32[]{:S(2)}) copy-start(bf16[128,4096]{1,0:T(8,128)(2,1)} %param.8) | copy-start | bytes 3145732
  7.2 76.3 %all-gather.3.cloned.1.call-start = ((), (), s32[]{:S(2)}) async-start(), calls=%async_computation.1 | async-start | bytes 7864320 | tf_op jit(solution)/shard_map/all_gather | solution.py:22
  10.6 1.1 copy-start.4
  11.7 4.7 %copy-start = (bf16[128,4096]{1,0:T(8,128)(2,1)}, bf16[128,4096]{1,0:T(8,128)(2,1)S(1)}, u32[]{:S(2)}) copy-start(bf16[128,4096]{1,0:T(8,128)(2,1)S(1)} %get-tuple-element.3) | copy-start | bytes 3145732
  16.3 190.3 %all-to-all-start = ((bf16[8,128,4096]{2,1,0:T(8,128)(2,1)}), bf16[8,128,4096]{2,1,0:T(8,128)(2,1)}, u32[]{:S(2)}, u32[]{:S(2)}) async-start(bf16[8,128,4096]{2,1,0:T(8,128)(2,1)} %stack.2), calls=%async_computation | async-start | bytes 16777216 | tf_op jit(solution)/shard_map/all_to_all | solution.py:26
  22.7 194.9 %all-gather.5.cloned.1.call-start = ((), (), s32[]{:S(2)}) async-start(), calls=%async_computation.2 | async-start | bytes 7864320 | tf_op jit(solution)/shard_map/all_gather | solution.py:23
  206.6 11.0 %copy-start.5 = (f32[768]{0:T(1024)S(1)}, f32[768]{0:T(1024)}, u32[]{:S(2)}) copy-start(f32[768]{0:T(1024)} %param.15) | copy-start | bytes 9220
  206.6 11.0 %copy-start.6 = (f32[768]{0:T(1024)S(1)}, f32[768]{0:T(1024)}, u32[]{:S(2)}) copy-start(f32[768]{0:T(1024)} %param.14) | copy-start | bytes 9220
Sparse Core Ops, SparseCore 0:
  10.7 72.7 all-gather.2
  85.3 70.0 all-gather.4
